TPU v7x, 32 devices: a whole 2x2x4 slice. The times are simulated.
32 devices in a mesh: grp: 2 (over x), ep: 16 (over z, y, core).
Axes of the slice: x: 2, y: 2, z: 4, core: 2. Of those that a mesh axis runs over, the one named last changes fastest.
Arguments:
- tokens: bfloat16 [4096, 2048], P(('grp', 'ep')), parts along dimension 0, may hold values from -6 to 6
- norm_gain: float32 [2048], replicated, may hold values from 0.1 to 1.9
- expert_ids: int32 [4096, 2], P(('grp', 'ep')), parts along dimension 0, may hold values from 0 to 3, as said below
- mix_weights: float32 [4096, 2], P(('grp', 'ep')), parts along dimension 0, may hold values from 0.2 to 1
- gate_weight: bfloat16 [2048, 28672], P(None, 'ep'), may hold values from -0.125 to 0.125
- up_weight: bfloat16 [2048, 28672], P(None, 'ep'), may hold values from -0.125 to 0.125
- down_weight: bfloat16 [28672, 2048], P('ep'), may hold values from -0.0625 to 0.0625
Outputs:
- mixed: bfloat16 [4096, 2048], P(('grp', 'ep')), parts along dimension 0
There are 2 independent parts, one for each index of `grp`. A program takes and returns all parts, laid end to end along the dimension named above; an argument that names none is the same for every part. Nothing has to cross between parts.
Inputs may be any that keep to these rules, and one draw needn't show every extreme that they name: `expert_ids`: each token names 2 different experts. In the rows of one device no expert is named by more than 80 rows, and in every draw each expert is named by exactly 80 rows of some device.
All inputs are finite; a program needn't handle non-finite values.
Results may differ from a plain program's by a relative error of at most 0.008.
Values may be sent and summed in bfloat16 or wider, within the bound.
A program may use at most 128 MiB of HBM per device.

v0:
```python
import jax
import jax.numpy as jnp
from jax import lax
from jax.sharding import PartitionSpec as P

TOP = 2
SPLIT = 4


def expert_ffn(arrived, gate_weight, up_weight, down_weight):
    width = arrived.shape[-1]
    inputs = arrived.reshape(-1, width)
    gate = jnp.dot(inputs, gate_weight, preferred_element_type=jnp.float32)
    upper = jnp.dot(inputs, up_weight, preferred_element_type=jnp.float32)
    hidden = (jax.nn.silu(gate) * upper).astype(jnp.bfloat16)
    result = jnp.dot(hidden, down_weight, preferred_element_type=jnp.float32).astype(jnp.bfloat16)
    return result.reshape(arrived.shape)


def local(tokens, norm_gain, expert_ids, mix_weights, gate_weight, up_weight, down_weight):
    n_dev = lax.axis_size("ep")
    experts = n_dev // SPLIT
    tok_rows, width = tokens.shape
    capacity = SPLIT * ((tok_rows * TOP * SPLIT * 5 // (4 * n_dev) + SPLIT - 1) // SPLIT)
    values = tokens.astype(jnp.float32)
    normed = (
        values * lax.rsqrt(jnp.mean(values * values, axis=-1, keepdims=True) + 1e-06) * norm_gain
    ).astype(jnp.bfloat16)
    flat_ids = expert_ids.reshape(-1)
    onehot = (flat_ids[:, None] == jnp.arange(experts, dtype=jnp.int32)[None, :]).astype(jnp.int32)
    before = jnp.cumsum(onehot, axis=0) - onehot
    slots = jnp.sum(before * onehot, axis=1).reshape(expert_ids.shape)
    target = expert_ids * capacity + slots
    places = jnp.arange(experts * capacity, dtype=jnp.int32)
    dispatch = jnp.any(places[:, None, None] == target[None, :, :], axis=2).astype(jnp.bfloat16)
    buffer = jnp.dot(dispatch, normed, preferred_element_type=jnp.float32).astype(jnp.bfloat16)
    buffer = buffer.reshape(experts, capacity, width)
    copies = jnp.repeat(buffer, SPLIT, axis=0)
    result = expert_ffn(
        lax.all_to_all(copies, "ep", split_axis=0, concat_axis=0, tiled=True),
        gate_weight,
        up_weight,
        down_weight,
    )
    returned = lax.all_to_all(result, "ep", split_axis=0, concat_axis=0, tiled=True)
    expert_out = jnp.sum(
        returned.reshape(experts, SPLIT, capacity, width).astype(jnp.float32), axis=1
    )
    expert_out = expert_out.reshape(experts * capacity, width)
    mixed = jnp.zeros((tok_rows, width), jnp.float32)
    for pick in range(TOP):
        mixed = mixed + mix_weights[:, pick : pick + 1] * jnp.take(
            expert_out, target[:, pick], axis=0
        )
    return mixed.astype(jnp.bfloat16)


def solution(mesh):
    in_specs = (
        P(("grp", "ep"), None),
        P(),
        P(("grp", "ep"), None),
        P(("grp", "ep"), None),
        P(None, "ep"),
        P(None, "ep"),
        P("ep", None),
    )
    out_specs = P(("grp", "ep"), None)
    return jax.shard_map(local, mesh=mesh, in_specs=in_specs, out_specs=out_specs, check_vma=False)
```

profile of v0, /device:TPU:13, one launch (start us, length us, event | category | flops | bytes accessed | tf_op | source)
XLA Modules:
  0.0 304.3 jit_solution(14560258273662790692)
XLA Ops:
  0.0 0.8 copy.30
  0.8 0.1 eq.43
  0.9 0.1 eq.39
  1.1 1.2 reduce-window.6
  2.3 0.1 slice.28
  2.4 0.1 copy.32
  2.5 0.1 copy.33
  2.6 0.1 add_bitcast_fusion
  2.7 0.1 reshape.54
  2.9 0.1 copy.34
  2.9 0.7 multiply_add_fusion
  3.7 1.2 fusion.4
  4.9 1.6 convolution_convert_fusion
  6.5 0.0 slice-start
  6.6 0.7 broadcast_in_dim.8
  7.2 0.0 slice-start.1
  7.2 121.3 %all_to_all.10 = bf16[16,80,2048]{2,1,0:T(8,128)(2,1)S(1)} all-to-all(bf16[16,80,2048]{2,1,0:T(8,128)(2,1)S(1)} %bitcast.45), channel_id=1, replica_groups=mesh['grp'=2,'ep'=16] {'ep'}, dimensions={0} | all-to-all | bytes 10485760 | tf_op jit(solution)/shard_map/all_to_all | solution.py:40
  128.5 0.0 copy-start
  128.5 2.3 copy-done
  130.8 0.0 slice-done
  130.8 0.0 slice-done.1
  130.8 12.0 %fusion.17 = f32[1280,1792]{1,0:T(8,128)} fusion(bf16[1280,2048]{1,0:T(8,128)(2,1)S(1)} %bitcast.47, bf16[2048,1792]{1,0:T(8,128)(2,1)S(1)} %bitcast.52), kind=kOutput, calls=%fused_computation.40 | convolution fusion | flops 9395240960 | bytes 21757952 | tf_op jit(solution)/shard_map/dot_general | solution.py:13
  142.8 30.7 %fusion.2 = bf16[1280,2048]{1,0:T(8,128)(2,1)} fusion(bf16[1792,2048]{1,0:T(8,128)(2,1)} %param.15, bf16[1280,2048]{1,0:T(8,128)(2,1)} %bitcast.48, bf16[2048,1792]{1,0:T(8,128)(2,1)} %param.14, f32[1280,1792]{1,0:T(8,128)} %fusion.17), kind=kOutput, calls=%fused_computation.6 | convolution fusion | flops 18806865920 | bytes 34340864 | tf_op jit(solution)/shard_map/dot_general | solution.py:16
  173.5 0.0 copy-start.1
  173.5 5.4 %all-to-all-start.1 = ((bf16[16,80,2048]{2,1,0:T(8,128)(2,1)}), bf16[16,80,2048]{2,1,0:T(8,128)(2,1)}, u32[]{:S(2)}, u32[]{:S(2)}) async-start(bf16[16,80,2048]{2,1,0:T(8,128)(2,1)} %bitcast.46), calls=%async_computation.1 | async-start | bytes 10485760 | tf_op jit(solution)/shard_map/all_to_all | solution.py:45
  179.0 0.0 copy-done.1
  179.0 114.9 %all-to-all-done.1 = bf16[16,80,2048]{2,1,0:T(8,128)(2,1)} async-done(((bf16[16,80,2048]{2,1,0:T(8,128)(2,1)}), bf16[16,80,2048]{2,1,0:T(8,128)(2,1)}, u32[]{:S(2)}, u32[]{:S(2)}) %all-to-all-start.1) | async-done | bytes 5242912 | tf_op jit(solution)/shard_map/all_to_all | solution.py:45
  293.9 3.8 %convert_reduce_fusion = f32[4,80,2048]{2,1,0:T(8,128)S(1)} fusion(bf16[16,80,2048]{2,1,0:T(8,128)(2,1)} %all-to-all-done.1), kind=kLoop, calls=%fused_computation.2 | loop fusion | flops 4587520 | bytes 7864320 | tf_op jit(solution)/shard_map/reduce_sum | solution.py:46
  297.7 1.9 gather_fusion.1
  299.7 2.0 gather_fusion
  301.7 2.6 fusion.8
  (10 shorter events, 0.1 us)
Async XLA Ops:
  6.5 124.3 %slice-start = ((s8[7340032]{0:T(1024)(128)(4,1)}), s8[4194304]{0:T(1024)(128)(4,1)S(1)}, s32[]{:S(2)}) async-start(s8[7340032]{0:T(1024)(128)(4,1)} %bitcast.51), calls=%async_computation.2 | async-start | bytes 8388608
  7.2 123.6 %slice-start.1 = ((s8[7340032]{0:T(1024)(128)(4,1)}), s8[3145728]{0:T(1024)(128)(4,1)S(1)}, s32[]{:S(2)}) async-start(s8[7340032]{0:T(1024)(128)(4,1)} %bitcast.51), calls=%async_computation.3 | async-start | bytes 6291456
  128.5 2.3 copy-start
  173.5 5.5 %copy-start.1 = (f32[128,2]{0,1:T(2,128)S(1)}, f32[128,2]{0,1:T(2,128)}, u32[]{:S(2)}) copy-start(f32[128,2]{0,1:T(2,128)} %param.12) | copy-start | bytes 3076
  173.5 120.4 %all-to-all-start.1 = ((bf16[16,80,2048]{2,1,0:T(8,128)(2,1)}), bf16[16,80,2048]{2,1,0:T(8,128)(2,1)}, u32[]{:S(2)}, u32[]{:S(2)}) async-start(bf16[16,80,2048]{2,1,0:T(8,128)(2,1)} %bitcast.46), calls=%async_computation.1 | async-start | bytes 10485760 | tf_op jit(solution)/shard_map/all_to_all | solution.py:45
where the time goes:
time: 305 us; the launch traced here: 304 us
  blocking collectives  121 us (40%)
  waiting for transfers between devices  115 us (38%)
  matrix products  44.4 us (15%)
  other arithmetic  9.8 us (3%)
  local copies, waits for them, and re-layouts  8.42 us (3%)
  starting transfers between devices  5.43 us (2%)
    all_to_all x1, blocking collectives, local(): lax.all_to_all(copies, 'ep', split_axis=0, concat_axis=0, tiled=True)  121 us
    all_to_all x1, waiting for transfers between devices, local(): lax.all_to_all(result, 'ep', split_axis=0, concat_axis=0, tiled=True)  115 us
    dot_general x1, matrix products, expert_ffn(): jnp.dot(hidden, down_weight, preferred_element_type=jnp.float32)  30.7 us
    dot_general x1, matrix products, expert_ffn(): gate = jnp.dot(inputs, gate_weight, preferred_element_type=jnp.float32)  12 us
  transfers between devices with their start and end apart: 1, of which 1 were waited for; matrix products, arithmetic and copies ran while one was open for 0% of the time, Pallas kernels for 0%

commit v1 on v0

v1 whole, which is shorter than its diff:
```python
import functools

import jax
import jax.numpy as jnp
from jax import lax
from jax.experimental import pallas as pl
from jax.experimental.pallas import tpu as pltpu
from jax.sharding import PartitionSpec as P

SPLIT = 4
f32, bf16 = jnp.float32, jnp.bfloat16


def tile_of(extent, most):
    tile = most
    while extent % tile:
        tile //= 2
    return tile


def kernel(
    experts,
    tok_ref, gain_ref, ids_ref, mix_ref, wg_hbm, wu_hbm, wd_hbm,
    out_ref,
    wg, wu, wd, normed, disp, xin, hid, part, r1, r2s, r2r, r3s, home, acc,
    w_sem, zs_sem, zr_sem, ys_sem, yr_sem, cs_sem, cr_sem, ds_sem, dr_sem,
    r1s_sem, r1r_sem, r2s_sem, r2r_sem, r3s_sem, r3r_sem,
):
    me = lax.axis_index("ep")
    z = me // SPLIT
    y = (me // 2) % 2
    c = me % 2
    rows, width = tok_ref.shape
    cap = disp.shape[1]
    ff = wg.shape[1]
    top = ids_ref.shape[1]
    at_y = {"ep": z * SPLIT + (1 - y) * 2 + c}
    at_c = {"ep": z * SPLIT + y * 2 + (1 - c)}
    mine = c * 2 + y
    other_y = c * 2 + 1 - y

    def peer(i):
        return z ^ i

    def at_z(i):
        return {"ep": peer(i) * SPLIT + y * 2 + c}

    def remote(src, dst, send, recv, where):
        return pltpu.make_async_remote_copy(
            src_ref=src, dst_ref=dst, send_sem=send, recv_sem=recv,
            device_id=where, device_id_type=pl.DeviceIdType.MESH,
        )

    ft = tile_of(ff, 256)
    nf = ff // ft
    dt = tile_of(width, 256)
    nd = width // dt

    def weight_gu(j):
        cols = pl.ds(pl.multiple_of(j * ft, ft), ft)
        return (
            pltpu.make_async_copy(wg_hbm.at[:, cols], wg.at[:, cols], w_sem.at[0, j]),
            pltpu.make_async_copy(wu_hbm.at[:, cols], wu.at[:, cols], w_sem.at[1, j]),
        )

    weight_d = pltpu.make_async_copy(wd_hbm, wd, w_sem.at[2, 0])

    barrier = pltpu.get_barrier_semaphore()
    for i in range(1, experts):
        pl.semaphore_signal(barrier, inc=1, device_id=at_z(i), device_id_type=pl.DeviceIdType.MESH)
    pl.semaphore_signal(barrier, inc=1, device_id=at_y, device_id_type=pl.DeviceIdType.MESH)
    pl.semaphore_signal(barrier, inc=1, device_id=at_c, device_id_type=pl.DeviceIdType.MESH)

    for j in range(nf):
        for copy in weight_gu(j):
            copy.start()
    weight_d.start()

    step = tile_of(rows, 16)

    @pl.loop(0, rows // step)
    def _(r):
        at = pl.ds(pl.multiple_of(r * step, step), step)
        values = tok_ref[at, :].astype(f32)
        scale = lax.rsqrt(jnp.mean(values * values, axis=-1, keepdims=True) + 1e-06)
        normed[at, :] = (values * scale * gain_ref[...]).astype(bf16)

    lanes = 128
    lane = lax.broadcasted_iota(jnp.int32, (rows, lanes), 1)
    named = ids_ref[:, 0:1] == lane
    for k in range(1, top):
        named = named | (ids_ref[:, k : k + 1] == lane)
    named = named.astype(f32).astype(bf16)
    first = lax.broadcasted_iota(jnp.int32, (rows, rows), 0)
    second = lax.broadcasted_iota(jnp.int32, (rows, rows), 1)
    upper = (first < second).astype(f32).astype(bf16)
    lower = (second < first).astype(f32).astype(bf16)
    eye = (second == first).astype(f32).astype(bf16)
    over_rows = (((0,), (0,)), ((), ()))
    rank_t = lax.dot_general(named, upper, over_rows, preferred_element_type=f32)
    named_t = lax.dot_general(named, eye, over_rows, preferred_element_type=f32)
    rank_t = jnp.where(named_t > 0.5, rank_t, -1.0)
    rank = jnp.dot(lower, named, preferred_element_type=f32)
    rank = jnp.where(named.astype(f32) > 0.5, rank, -1.0)
    expert_row = lax.broadcasted_iota(jnp.int32, (lanes, rows), 0)

    def dispatch(e, dst):
        slot = jnp.sum(jnp.where(expert_row == e, rank_t, 0.0), axis=0, keepdims=True)
        place = lax.broadcasted_iota(jnp.int32, (cap, rows), 0)
        pick = (place == slot.astype(jnp.int32)).astype(f32).astype(bf16)
        wide = tile_of(width, 512)
        for n in range(width // wide):
            cols = slice(n * wide, (n + 1) * wide)
            dst[:, cols] = jnp.dot(pick, normed[:, cols], preferred_element_type=f32).astype(bf16)

    def z_copy(i):
        return remote(disp.at[i], xin.at[z, mine], zs_sem.at[i], zr_sem.at[z], at_z(i))

    def z_arrival(i):
        return remote(disp.at[i], xin.at[peer(i), mine], zs_sem.at[i], zr_sem.at[peer(i)], at_z(i))

    def y_copy(i):
        slot = xin.at[peer(i), mine]
        return remote(slot, slot, ys_sem.at[i], yr_sem.at[i], at_y)

    def y_arrival(i):
        slot = xin.at[peer(i), other_y]
        return remote(slot, slot, ys_sem.at[i], yr_sem.at[i], at_y)

    def c_copy(i):
        slot = xin.at[peer(i), mine]
        return remote(slot, slot, cs_sem.at[i], cr_sem.at[i], at_c)

    def c_arrival(i):
        slot = xin.at[peer(i), (1 - c) * 2 + y]
        return remote(slot, slot, cs_sem.at[i], cr_sem.at[i], at_c)

    def d_copy(i):
        slot = xin.at[peer(i), other_y]
        return remote(slot, slot, ds_sem.at[i], dr_sem.at[i], at_c)

    def d_arrival(i):
        slot = xin.at[peer(i), (1 - c) * 2 + 1 - y]
        return remote(slot, slot, ds_sem.at[i], dr_sem.at[i], at_c)

    def r1_copy(i):
        return remote(part.at[i, 1 - c], r1.at[i], r1s_sem.at[i], r1r_sem.at[i], at_c)

    def r2_copy(i):
        return remote(r2s.at[i], r2r.at[i], r2s_sem.at[i], r2r_sem.at[i], at_y)

    def r3_copy(i):
        return remote(r3s.at[i], home.at[z], r3s_sem.at[i], r3r_sem.at[z], at_z(i))

    def r3_arrival(i):
        return remote(r3s.at[i], home.at[peer(i)], r3s_sem.at[i], r3r_sem.at[peer(i)], at_z(i))

    dispatch(z, xin.at[z, mine])
    pl.semaphore_wait(barrier, experts + 1)
    y_copy(0).start()
    c_copy(0).start()

    @pl.loop(1, experts)
    def _(i):
        dispatch(peer(i), disp.at[i])
        z_copy(i).start()

    acc[...] = jnp.zeros_like(acc)

    def gate_up(i, low, high):
        @pl.loop(low, high)
        def _(j):
            @pl.when(i == 0)
            def _():
                for copy in weight_gu(j):
                    copy.wait()

            cols = pl.ds(pl.multiple_of(j * ft, ft), ft)
            inputs = xin[peer(i)].reshape(SPLIT * cap, width)
            gate = jnp.dot(inputs, wg[:, cols], preferred_element_type=f32)
            up = jnp.dot(inputs, wu[:, cols], preferred_element_type=f32)
            hid[:, cols] = (gate / (1.0 + jnp.exp(-gate)) * up).astype(bf16)

    def down(i):
        @pl.when(i == 0)
        def _():
            weight_d.wait()

        @pl.loop(0, nd)
        def _(j):
            cols = pl.ds(pl.multiple_of(j * dt, dt), dt)
            res = jnp.dot(hid[...], wd[:, cols], preferred_element_type=f32).astype(bf16)
            part[i, :, :, :, cols] = res.reshape(2, 2, cap, dt)

    def reduce_chip(i):
        r1_copy(i).wait_recv()

        @pl.loop(0, cap // 16)
        def _(r):
            at = pl.ds(pl.multiple_of(r * 16, 16), 16)
            r2s[i, at, :] = (
                part[i, c, 1 - y, at, :].astype(f32) + r1[i, 1 - y, at, :].astype(f32)
            ).astype(bf16)

        r2_copy(i).start()

    def reduce_group(i):
        r2_copy(i).wait_recv()

        def total(at):
            return (
                part[i, c, y, at, :].astype(f32)
                + r1[i, y, at, :].astype(f32)
                + r2r[i, at, :].astype(f32)
            ).astype(bf16)

        @pl.loop(0, cap // 16)
        def _(r):
            at = pl.ds(pl.multiple_of(r * 16, 16), 16)

            @pl.when(i == 0)
            def _():
                home[z, at, :] = total(at)

            @pl.when(i > 0)
            def _():
                r3s[i, at, :] = total(at)

        @pl.when(i > 0)
        def _():
            r3_copy(i).start()

    @pl.loop(0, experts)
    def _(i):
        y_arrival(i).wait_recv()
        d_copy(i).start()
        c_arrival(i).wait_recv()
        d_arrival(i).wait_recv()
        half = (nf + 1) // 2
        gate_up(i, 0, half)

        @pl.when(i + 1 < experts)
        def _():
            z_arrival(i + 1).wait_recv()
            y_copy(i + 1).start()
            c_copy(i + 1).start()

        gate_up(i, half, nf)

        @pl.when(i > 0)
        def _():
            reduce_chip(i - 1)

        down(i)
        r1_copy(i).start()

        @pl.when(i > 0)
        def _():
            reduce_group(i - 1)

    reduce_chip(experts - 1)
    reduce_group(experts - 1)

    @pl.loop(0, experts)
    def _(i):
        e = peer(i)

        @pl.when(i > 0)
        def _():
            r3_arrival(i).wait_recv()

        slot = jnp.sum(jnp.where(lane == e, rank, 0.0), axis=1, keepdims=True)
        place = lax.broadcasted_iota(jnp.int32, (rows, cap), 1)
        pick = (place == slot.astype(jnp.int32)).astype(f32).astype(bf16)
        weight = jnp.where(ids_ref[:, 0:1] == e, mix_ref[:, 0:1], 0.0)
        for k in range(1, top):
            weight = weight + jnp.where(ids_ref[:, k : k + 1] == e, mix_ref[:, k : k + 1], 0.0)
        wide = tile_of(width, 512)
        for n in range(width // wide):
            cols = slice(n * wide, (n + 1) * wide)
            acc[:, cols] += weight * jnp.dot(pick, home[e, :, cols], preferred_element_type=f32)

    out_ref[...] = acc[...].astype(bf16)

    @pl.loop(0, experts)
    def _(i):
        @pl.when(i > 0)
        def _():
            z_copy(i).wait_send()
            r3_copy(i).wait_send()

        y_copy(i).wait_send()
        c_copy(i).wait_send()
        d_copy(i).wait_send()
        r1_copy(i).wait_send()
        r2_copy(i).wait_send()


def local(tokens, norm_gain, expert_ids, mix_weights, gate_weight, up_weight, down_weight):
    n_dev = lax.axis_size("ep")
    experts = n_dev // SPLIT
    rows, width = tokens.shape
    top = expert_ids.shape[1]
    ff = gate_weight.shape[1]
    cap = (rows * top * SPLIT * 5 + 4 * n_dev - 1) // (4 * n_dev)
    cap = (cap + 15) // 16 * 16
    nf = ff // tile_of(ff, 256)
    dma = pltpu.SemaphoreType.DMA
    vmem = pl.BlockSpec(memory_space=pltpu.VMEM)
    hbm = pl.BlockSpec(memory_space=pl.ANY)
    block = (cap, width)
    return pl.pallas_call(
        functools.partial(kernel, experts),
        out_shape=jax.ShapeDtypeStruct((rows, width), bf16),
        in_specs=[vmem, vmem, vmem, vmem, hbm, hbm, hbm],
        out_specs=vmem,
        scratch_shapes=[
            pltpu.VMEM((width, ff), bf16),
            pltpu.VMEM((width, ff), bf16),
            pltpu.VMEM((ff, width), bf16),
            pltpu.VMEM((rows, width), bf16),
            pltpu.VMEM((experts,) + block, bf16),
            pltpu.VMEM((experts, SPLIT) + block, bf16),
            pltpu.VMEM((SPLIT * cap, ff), bf16),
            pltpu.VMEM((experts, 2, 2) + block, bf16),
            pltpu.VMEM((experts, 2) + block, bf16),
            pltpu.VMEM((experts,) + block, bf16),
            pltpu.VMEM((experts,) + block, bf16),
            pltpu.VMEM((experts,) + block, bf16),
            pltpu.VMEM((experts,) + block, bf16),
            pltpu.VMEM((rows, width), f32),
            dma((3, nf)),
        ] + [dma((experts,))] * 14,
        compiler_params=pltpu.CompilerParams(
            collective_id=0, has_side_effects=True, vmem_limit_bytes=64 * 1024 * 1024 - 65536,
        ),
    )(tokens, norm_gain.reshape(1, width), expert_ids, mix_weights, gate_weight, up_weight, down_weight)


def solution(mesh):
    in_specs = (
        P(("grp", "ep"), None),
        P(),
        P(("grp", "ep"), None),
        P(("grp", "ep"), None),
        P(None, "ep"),
        P(None, "ep"),
        P("ep", None),
    )
    out_specs = P(("grp", "ep"), None)
    return jax.shard_map(local, mesh=mesh, in_specs=in_specs, out_specs=out_specs, check_vma=False)
```

time: 305 us -> 120 us (0.39)
  blocking collectives: 121 us -> 0 us
  waiting for transfers between devices: 115 us -> 0 us
  Pallas kernels: 0 us -> 114 us
  matrix products: 44.4 us -> 0 us
  other arithmetic: 9.8 us -> 0 us
  starting transfers between devices: 5.43 us -> 0 us
  local copies, waits for them, and re-layouts: 8.42 us -> 4.7 us
    all_to_all x1 -> x0, blocking collectives: 121 us -> none  [local(): lax.all_to_all(copies, 'ep', split_axis=0, concat_axis=0, tiled=True)]
    all_to_all x1 -> x0, waiting for transfers between devices: 115 us -> none  [local(): lax.all_to_all(result, 'ep', split_axis=0, concat_axis=0, tiled=True)]
    pallas_call x0 -> x1, Pallas kernels: none -> 114 us  [local(): pl.pallas_call(functools.partial(kernel, experts), out_shape=jax.ShapeDty...]
    dot_general x3 -> x0, matrix products: 44.4 us -> none  [the longest x1 30.7 us: expert_ffn(): jnp.dot(hidden, down_weight, preferred_element_type=jnp.float32)]
    all_to_all x1 -> x0, starting transfers between devices: 5.43 us -> none  [local(): lax.all_to_all(result, 'ep', split_axis=0, concat_axis=0, tiled=True)]
    reduce_sum x3 -> x0, other arithmetic: 5.06 us -> none  [the longest x1 3.81 us: local(): jnp.sum(returned.reshape(experts, SPLIT, capacity, width).astype(jnp.floa...]
    gather x2 -> x0, local copies, waits for them, and re-layouts: 3.92 us -> none  [local(): jnp.take(expert_out, target[:, pick], axis=0)]
  transfers between devices with their start and end apart: 1 -> 0, of which waited for: 1 -> 0; matrix products, arithmetic and copies ran while one was open for 0% -> 0% of each run, Pallas kernels for 0% -> 0%
where the time goes in v1:
time: 120 us; the launch traced here: 118 us
  Pallas kernels  114 us (95%)
  local copies, waits for them, and re-layouts  4.7 us (4%)
    pallas_call x1, Pallas kernels, local(): pl.pallas_call(functools.partial(kernel, experts), out_shape=jax.ShapeDty...  114 us
    unnamed x3, local copies, waits for them, and re-layouts  4.7 us

profile of v1, /device:TPU:13, one launch (start us, length us, event | category | flops | bytes accessed | tf_op | source)
XLA Modules:
  0.0 118.3 jit_solution(6396144118493988909)
XLA Ops:
  0.0 1.4 %copy.8.ids_ref = s32[128,2]{1,0:T(8,128)} copy(s32[128,2]{0,1:T(2,128)} %param.9) | data formatting | bytes 2048 | tf_op args[2]
  1.4 1.4 %copy.9.mix_ref = f32[128,2]{1,0:T(8,128)} copy(f32[128,2]{0,1:T(2,128)} %param.10) | data formatting | bytes 2048 | tf_op args[3]
  2.8 113.6 %shard_map.73 = bf16[128,2048]{1,0:T(8,128)(2,1)} custom-call(bf16[128,2048]{1,0:T(8,128)(2,1)} %tok_ref.1, f32[1,2048]{1,0:T(1,128)} %bitcast.1, s32[128,2]{1,0:T(8,128)} %copy.8.ids_ref, f32[128,2]{1,0:T(8,128)} %copy.9.mix_ref, bf16[2048,1792]{1,0:T(8,128)(2,1)} %wg_hbm.1, bf16[2048,1792]{1,0:T(8,128)(2,1)} %wu_hbm.1, bf16[1792,2048]{1,0:T(8,128)(2,1)} %wd_hbm.1), custom_call_target="tpu_custom_call" | custom-call | tf_op jit(solution)/shard_map/pallas_call | solution.py:312
  116.4 1.9 %copy.11 = bf16[128,2048]{1,0:T(8,128)(2,1)} copy(bf16[128,2048]{1,0:T(8,128)(2,1)} %shard_map.73) | data formatting | bytes 1048576

commit v2 on v1

v2 whole, which is shorter than its diff:
```python
import functools

import jax
import jax.numpy as jnp
from jax import lax
from jax.experimental import pallas as pl
from jax.experimental.pallas import tpu as pltpu
from jax.sharding import PartitionSpec as P

SPLIT = 4
CHUNK = 16
f32, bf16 = jnp.float32, jnp.bfloat16


def tile_of(extent, most):
    tile = most
    while extent % tile:
        tile //= 2
    return tile


def kernel(
    experts,
    tok_ref, gain_ref, ids_ref, mix_ref, wg_hbm, wu_hbm, wd_hbm,
    out_ref,
    wg, wu, wd, normed, disp, xin, hid, part, r1, r2s, r2r, r3s, home, acc,
    w_sem, zs_sem, zr_sem, ys_sem, yr_sem, cs_sem, cr_sem, ds_sem, dr_sem,
    r1s_sem, r1r_sem, r2s_sem, r2r_sem, r3s_sem, r3r_sem,
):
    me = lax.axis_index("ep")
    z = me // SPLIT
    y = (me // 2) % 2
    c = me % 2
    rows, width = tok_ref.shape
    cap = disp.shape[1]
    nq = cap // CHUNK
    ff = wg.shape[1]
    top = ids_ref.shape[0]
    at_y = {"ep": z * SPLIT + (1 - y) * 2 + c}
    at_c = {"ep": z * SPLIT + y * 2 + (1 - c)}
    mine = c * 2 + y
    other_y = c * 2 + 1 - y
    other_c = (1 - c) * 2 + y
    other_yc = (1 - c) * 2 + 1 - y

    def peer(k):
        shift = jnp.where(k == 0, 0, (k + experts // 2 - 2) % (experts - 1) + 1)
        return z ^ shift

    def at_z(k):
        return {"ep": peer(k) * SPLIT + y * 2 + c}

    def remote(src, dst, send, recv, where):
        return pltpu.make_async_remote_copy(
            src_ref=src, dst_ref=dst, send_sem=send, recv_sem=recv,
            device_id=where, device_id_type=pl.DeviceIdType.MESH,
        )

    def chunk(q):
        return pl.ds(pl.multiple_of(q * CHUNK, CHUNK), CHUNK)

    ft = tile_of(ff, 256)
    nf = ff // ft
    dt = tile_of(width, 256)
    nd = width // dt

    def weight_gu(j):
        cols = pl.ds(pl.multiple_of(j * ft, ft), ft)
        return (
            pltpu.make_async_copy(wg_hbm.at[:, cols], wg.at[:, cols], w_sem.at[0, j]),
            pltpu.make_async_copy(wu_hbm.at[:, cols], wu.at[:, cols], w_sem.at[1, j]),
        )

    weight_d = pltpu.make_async_copy(wd_hbm, wd, w_sem.at[2, 0])

    barrier = pltpu.get_barrier_semaphore()

    for k in range(1, experts):
        pl.semaphore_signal(barrier, inc=1, device_id=at_z(k), device_id_type=pl.DeviceIdType.MESH)
    pl.semaphore_signal(barrier, inc=1, device_id=at_y, device_id_type=pl.DeviceIdType.MESH)
    pl.semaphore_signal(barrier, inc=1, device_id=at_c, device_id_type=pl.DeviceIdType.MESH)

    for j in range(nf):
        for copy in weight_gu(j):
            copy.start()
    weight_d.start()

    step = tile_of(rows, 16)

    @pl.loop(0, rows // step)
    def _(r):
        at = pl.ds(pl.multiple_of(r * step, step), step)
        values = tok_ref[at, :].astype(f32)
        scale = lax.rsqrt(jnp.mean(values * values, axis=-1, keepdims=True) + 1e-06)
        normed[at, :] = (values * scale * gain_ref[...]).astype(bf16)

    lanes = 128
    expert_row = lax.broadcasted_iota(jnp.int32, (lanes, rows), 0)
    named = ids_ref[0:1, :] == expert_row
    weight_t = jnp.where(named, mix_ref[0:1, :], 0.0)
    for k in range(1, top):
        hit = ids_ref[k : k + 1, :] == expert_row
        named = named | hit
        weight_t = weight_t + jnp.where(hit, mix_ref[k : k + 1, :], 0.0)
    named = named.astype(f32)
    first = lax.broadcasted_iota(jnp.int32, (rows, rows), 0)
    second = lax.broadcasted_iota(jnp.int32, (rows, rows), 1)
    upper = (first < second).astype(f32).astype(bf16)
    rank_t = jnp.dot(named.astype(bf16), upper, preferred_element_type=f32)
    rank_t = jnp.where(named > 0.5, rank_t, -1.0)
    rank = jnp.transpose(rank_t)
    weight_c = jnp.transpose(weight_t)
    lane = lax.broadcasted_iota(jnp.int32, (rows, lanes), 1)

    def dispatch(e, dst):
        slot = jnp.sum(jnp.where(expert_row == e, rank_t, 0.0), axis=0, keepdims=True)
        place = lax.broadcasted_iota(jnp.int32, (cap, rows), 0)
        pick = (place == slot.astype(jnp.int32)).astype(f32).astype(bf16)
        wide = tile_of(width, 512)
        for n in range(width // wide):
            cols = slice(n * wide, (n + 1) * wide)
            dst[:, cols] = jnp.dot(pick, normed[:, cols], preferred_element_type=f32).astype(bf16)

    def z_copy(k, q):
        return remote(disp.at[k, chunk(q)], xin.at[z, mine, chunk(q)], zs_sem.at[k, q], zr_sem.at[z, q], at_z(k))

    def z_arrival(k, q):
        p = peer(k)
        return remote(disp.at[k, chunk(q)], xin.at[p, mine, chunk(q)], zs_sem.at[k, q], zr_sem.at[p, q], at_z(k))

    def in_group(sub, send, recv, where):
        def make(k, q):
            slot = xin.at[peer(k), sub, chunk(q)]
            return remote(slot, slot, send.at[k, q], recv.at[k, q], where)

        return make

    y_copy = in_group(mine, ys_sem, yr_sem, at_y)
    y_arrival = in_group(other_y, ys_sem, yr_sem, at_y)
    c_copy = in_group(mine, cs_sem, cr_sem, at_c)
    c_arrival = in_group(other_c, cs_sem, cr_sem, at_c)
    d_copy = in_group(other_y, ds_sem, dr_sem, at_c)
    d_arrival = in_group(other_yc, ds_sem, dr_sem, at_c)

    def r1_copy(k, v, q):
        return remote(
            part.at[k, 1 - c, v, chunk(q)], r1.at[k, v, chunk(q)], r1s_sem.at[k, v, q], r1r_sem.at[k, v, q], at_c
        )

    def r2_copy(k, q):
        return remote(r2s.at[k, chunk(q)], r2r.at[k, chunk(q)], r2s_sem.at[k, q], r2r_sem.at[k, q], at_y)

    def r3_copy(k, q):
        return remote(r3s.at[k, chunk(q)], home.at[z, chunk(q)], r3s_sem.at[k, q], r3r_sem.at[z, q], at_z(k))

    def r3_arrival(k, q):
        p = peer(k)
        return remote(r3s.at[k, chunk(q)], home.at[p, chunk(q)], r3s_sem.at[k, q], r3r_sem.at[p, q], at_z(k))

    def forward_z(k, q):
        @pl.when(k > 0)
        def _():
            z_arrival(k, q).wait_recv()

        y_copy(k, q).start()
        c_copy(k, q).start()

    def forward_y(k, q):
        y_arrival(k, q).wait_recv()
        d_copy(k, q).start()

    def reduce_chip(k, q):
        at = chunk(q)
        r1_copy(k, 1 - y, q).wait_recv()
        r2s[k, at, :] = (part[k, c, 1 - y, at, :].astype(f32) + r1[k, 1 - y, at, :].astype(f32)).astype(bf16)
        r2_copy(k, q).start()

    def reduce_group(k, q):
        @pl.when(q < nq)
        def _():
            at = chunk(q)
            r1_copy(k, y, q).wait_recv()
            r2_copy(k, q).wait_recv()
            total = (
                part[k, c, y, at, :].astype(f32) + r1[k, y, at, :].astype(f32) + r2r[k, at, :].astype(f32)
            ).astype(bf16)

            @pl.when(k == 0)
            def _():
                home[z, at, :] = total

            @pl.when(k > 0)
            def _():
                r3s[k, at, :] = total
                r3_copy(k, q).start()

    dispatch(z, xin.at[z, mine])
    pl.semaphore_wait(barrier, experts + 1)

    @pl.loop(0, nq)
    def _(q):
        forward_z(0, q)

    @pl.loop(1, experts)
    def _(k):
        dispatch(peer(k), disp.at[k])

        @pl.loop(0, nq)
        def _(q):
            z_copy(k, q).start()

    acc[...] = jnp.zeros_like(acc)

    def gate_up(k, j):
        @pl.when(k == 0)
        def _():
            for copy in weight_gu(j):
                copy.wait()

        cols = pl.ds(pl.multiple_of(j * ft, ft), ft)
        inputs = xin[peer(k)].reshape(SPLIT * cap, width)
        gate = jnp.dot(inputs, wg[:, cols], preferred_element_type=f32)
        up = jnp.dot(inputs, wu[:, cols], preferred_element_type=f32)
        hid[:, cols] = (gate / (1.0 + jnp.exp(-gate)) * up).astype(bf16)

    def down(k, j):
        cols = pl.ds(pl.multiple_of(j * dt, dt), dt)
        res = jnp.dot(hid[...], wd[:, cols], preferred_element_type=f32).astype(bf16)
        part[k, :, :, :, cols] = res.reshape(2, 2, cap, dt)

    early = 2

    @pl.loop(0, nq)
    def _(q):
        forward_y(0, q)

        @pl.when(q < early)
        def _():
            forward_z(1, q)

    @pl.loop(0, experts)
    def _(k):
        @pl.loop(0, nq)
        def _(q):
            c_arrival(k, q).wait_recv()

        @pl.loop(0, nq)
        def _(q):
            d_arrival(k, q).wait_recv()

        @pl.loop(0, max(nf, nq))
        def _(j):
            @pl.when(j < nf)
            def _():
                gate_up(k, j)

            @pl.when((j < nq) & (k + 1 < experts) & ((k > 0) | (j >= early)))
            def _():
                forward_z(k + 1, j)

            @pl.when((j < nq) & (k > 0))
            def _():
                reduce_chip(k - 1, j)

        @pl.when(k == 0)
        def _():
            weight_d.wait()

        @pl.loop(0, max(nd, nq))
        def _(j):
            @pl.when(j < nd)
            def _():
                down(k, j)

            @pl.when((j < nq) & (k + 1 < experts))
            def _():
                forward_y(k + 1, j)

            @pl.when((j < nq) & (k > 0))
            def _():
                reduce_group(k - 1, j)

        for side in (1 - y, y):

            @pl.loop(0, nq)
            def _(q):
                r1_copy(k, side, q).start()

    @pl.loop(0, nq)
    def _(q):
        reduce_chip(experts - 1, q)

    @pl.loop(0, nq)
    def _(q):
        reduce_group(experts - 1, q)

    @pl.loop(0, experts)
    def _(k):
        e = peer(k)

        @pl.when(k > 0)
        def _():
            @pl.loop(0, nq)
            def _(q):
                r3_arrival(k, q).wait_recv()

        slot = jnp.sum(jnp.where(lane == e, rank, 0.0), axis=1, keepdims=True)
        weight = jnp.sum(jnp.where(lane == e, weight_c, 0.0), axis=1, keepdims=True)
        place = lax.broadcasted_iota(jnp.int32, (rows, cap), 1)
        pick = (place == slot.astype(jnp.int32)).astype(f32).astype(bf16)
        wide = tile_of(width, 512)
        for n in range(width // wide):
            cols = slice(n * wide, (n + 1) * wide)
            acc[:, cols] += weight * jnp.dot(pick, home[e, :, cols], preferred_element_type=f32)

    out_ref[...] = acc[...].astype(bf16)

    @pl.loop(0, experts)
    def _(k):
        @pl.when(k > 0)
        def _():
            @pl.loop(0, nq)
            def _(q):
                z_copy(k, q).wait_send()

            @pl.loop(0, nq)
            def _(q):
                r3_copy(k, q).wait_send()

        @pl.loop(0, nq)
        def _(q):
            y_copy(k, q).wait_send()
            c_copy(k, q).wait_send()

        @pl.loop(0, nq)
        def _(q):
            d_copy(k, q).wait_send()
            r2_copy(k, q).wait_send()

        for v in range(2):
            @pl.loop(0, nq)
            def _(q):
                r1_copy(k, v, q).wait_send()


def local(tokens, norm_gain, expert_ids, mix_weights, gate_weight, up_weight, down_weight):
    n_dev = lax.axis_size("ep")
    experts = n_dev // SPLIT
    rows, width = tokens.shape
    top = expert_ids.shape[1]
    ff = gate_weight.shape[1]
    cap = (rows * top * SPLIT * 5 + 4 * n_dev - 1) // (4 * n_dev)
    cap = (cap + CHUNK - 1) // CHUNK * CHUNK
    nq = cap // CHUNK
    nf = ff // tile_of(ff, 256)
    dma = pltpu.SemaphoreType.DMA
    vmem = pl.BlockSpec(memory_space=pltpu.VMEM)
    hbm = pl.BlockSpec(memory_space=pl.ANY)
    block = (cap, width)
    return pl.pallas_call(
        functools.partial(kernel, experts),
        out_shape=jax.ShapeDtypeStruct((rows, width), bf16),
        in_specs=[vmem, vmem, vmem, vmem, hbm, hbm, hbm],
        out_specs=vmem,
        scratch_shapes=[
            pltpu.VMEM((width, ff), bf16),
            pltpu.VMEM((width, ff), bf16),
            pltpu.VMEM((ff, width), bf16),
            pltpu.VMEM((rows, width), bf16),
            pltpu.VMEM((experts,) + block, bf16),
            pltpu.VMEM((experts, SPLIT) + block, bf16),
            pltpu.VMEM((SPLIT * cap, ff), bf16),
            pltpu.VMEM((experts, 2, 2) + block, bf16),
            pltpu.VMEM((experts, 2) + block, bf16),
            pltpu.VMEM((experts,) + block, bf16),
            pltpu.VMEM((experts,) + block, bf16),
            pltpu.VMEM((experts,) + block, bf16),
            pltpu.VMEM((experts,) + block, bf16),
            pltpu.VMEM((rows, width), f32),
            dma((3, nf)),
        ] + [dma((experts, nq))] * 8 + [dma((experts, 2, nq))] * 2 + [dma((experts, nq))] * 4,
        compiler_params=pltpu.CompilerParams(
            collective_id=0, has_side_effects=True, vmem_limit_bytes=64 * 1024 * 1024 - 65536,
        ),
    )(tokens, norm_gain.reshape(1, width), expert_ids.T, mix_weights.T, gate_weight, up_weight, down_weight)


def solution(mesh):
    in_specs = (
        P(("grp", "ep"), None),
        P(),
        P(("grp", "ep"), None),
        P(("grp", "ep"), None),
        P(None, "ep"),
        P(None, "ep"),
        P("ep", None),
    )
    out_specs = P(("grp", "ep"), None)
    return jax.shard_map(local, mesh=mesh, in_specs=in_specs, out_specs=out_specs, check_vma=False)
```

time: 120 us -> 105 us (0.88)
  Pallas kernels: 114 us -> 103 us
  local copies, waits for them, and re-layouts: 4.7 us -> 1.88 us
    pallas_call x1, Pallas kernels: 114 us -> 103 us  [local(): pl.pallas_call(functools.partial(kernel, experts), out_shape=jax.ShapeDty...]
    unnamed x3 -> x1, local copies, waits for them, and re-layouts: 4.7 us -> 1.88 us
where the time goes in v2:
time: 105 us; the launch traced here: 104 us
  Pallas kernels  103 us (98%)
  local copies, waits for them, and re-layouts  1.88 us (2%)
    pallas_call x1, Pallas kernels, local(): pl.pallas_call(functools.partial(kernel, experts), out_shape=jax.ShapeDty...  103 us

profile of v2, /device:TPU:13, one launch (start us, length us, event | category | flops | bytes accessed | tf_op | source)
XLA Modules:
  0.0 104.4 jit_solution(5193545179753040178)
XLA Ops:
  0.0 102.5 %shard_map.73 = bf16[128,2048]{1,0:T(8,128)(2,1)} custom-call(bf16[128,2048]{1,0:T(8,128)(2,1)} %tok_ref.1, f32[1,2048]{1,0:T(1,128)} %bitcast.3, s32[2,128]{1,0:T(2,128)} %bitcast.4, f32[2,128]{1,0:T(2,128)} %bitcast.5, bf16[2048,1792]{1,0:T(8,128)(2,1)} %wg_hbm.1, bf16[2048,1792]{1,0:T(8,128)(2,1)} %wu_hbm.1, bf16[1792,2048]{1,0:T(8,128)(2,1)} %wd_hbm.1), custom_call_target="tpu_custom_call" | custom-call | tf_op jit(solution)/shard_map/pallas_call | solution.py:360
  102.5 1.9 %copy.9 = bf16[128,2048]{1,0:T(8,128)(2,1)} copy(bf16[128,2048]{1,0:T(8,128)(2,1)} %shard_map.73) | data formatting | bytes 1048576
